TPU v7x, 256 devices: a whole 4x4x8 slice. The times are simulated.
256 devices in a mesh: sp: 32 (over z, y), tp: 8 (over x, core).
Axes of the slice: x: 4, y: 4, z: 8, core: 2. Of those that a mesh axis runs over, the one named last changes fastest.
Arguments:
- tokens: bfloat16 [4, 16384, 2048], P(None, ('sp', 'tp')), may hold values from -6 to 6
- in_gain: float32 [2048], replicated, may hold values from 0.1 to 1.9
- query_weight: bfloat16 [2048, 1024], P(None, 'tp'), may hold values from -0.125 to 0.125
- key_weight: bfloat16 [2048, 1024], P(None, 'tp'), may hold values from -0.125 to 0.125
- value_weight: bfloat16 [2048, 1024], P(None, 'tp'), may hold values from -0.125 to 0.125
- gate_weight: bfloat16 [2048, 1024], P(None, 'tp'), may hold values from -0.125 to 0.125
- log_decay: float32 [8], P('tp'), may hold values from -0.034 to 0, as said below
- norm_gain: float32 [1024], P('tp'), may hold values from 0.1 to 1.9
- out_weight: bfloat16 [1024, 2048], replicated, may hold values from -0.1875 to 0.1875
- post_gain: float32 [2048], replicated, may hold values from 0.1 to 1.9
Outputs:
- mixed: bfloat16 [4, 16384, 2048], P(None, ('sp', 'tp'))
Inputs may be any that keep to these rules, and one draw needn't show every extreme that they name: `log_decay`: every entry is negative; some heads keep a tenth or more of their memory over 16384 positions, others lose most of it within 30 to 100 positions.
All inputs are finite; a program needn't handle non-finite values.
Results may differ from a plain program's by a relative error of at most 0.015.
Values may be sent and summed in bfloat16 or wider, within the bound.
A program may use at most 64 MiB of HBM per device.

v0:
```python
import jax
import jax.numpy as jnp
from jax import lax
from jax.sharding import Mesh
from jax.sharding import PartitionSpec as P

HEAD_DIM = 128
BLOCK = 128
SP = ("sp_0", "sp_1")
SP_TP = ("sp_0", "sp_1", "tp")
rms_eps = 1e-06
group_eps = 1e-05
rope_base = 10000.0


def neutral_like(shard, identity):
    return jax.tree.map(
        lambda part, zero: jnp.zeros_like(part) + jnp.asarray(zero, part.dtype), shard, identity
    )


def entering(shard, axes, combine, identity):
    before = start = neutral_like(shard, identity)
    running = shard
    for axis in reversed(axes):
        length, mine = (lax.axis_size(axis), lax.axis_index(axis))
        pieces = jax.tree.map(lambda part: lax.all_gather(part, axis), running)
        inside, running = (start, start)
        for k in range(length):
            passed = k < mine
            running = combine(running, jax.tree.map(lambda part: part[k], pieces))
            inside = jax.tree.map(lambda new, old: jnp.where(passed, new, old), running, inside)
        before = combine(inside, before)
    return before


def rotate(values, positions):
    half_dim = values.shape[-1] // 2
    inverse = rope_base ** (-jnp.arange(half_dim, dtype=jnp.float32) / half_dim)
    angles = positions.astype(jnp.float32)[:, None] * inverse[None, :]
    cosine = jnp.cos(angles)
    sine_part = jnp.sin(angles)
    first_half = values[..., :half_dim].astype(jnp.float32)
    second = values[..., half_dim:].astype(jnp.float32)
    return jnp.concatenate(
        [first_half * cosine - second * sine_part, first_half * sine_part + second * cosine],
        axis=-1,
    )


def local_pass(queries, key_rows, values, log_decay):
    seq_count, head_count, length, head_width = queries.shape
    block_count = length // BLOCK
    offsets = jnp.arange(BLOCK, dtype=jnp.float32)
    distance = offsets[:, None] - offsets[None, :]
    rate_col = log_decay[:, None, None]
    inside = jnp.where(distance >= 0, jnp.exp(rate_col * jnp.maximum(distance, 0.0)), 0.0)
    query_scale = jnp.exp(log_decay[:, None] * (offsets + 1.0))[..., None]
    key_scale = jnp.exp(log_decay[:, None] * (BLOCK - 1.0 - offsets))[..., None]
    block_decay = jnp.exp(log_decay * BLOCK)[:, None, None]

    def to_blocks(arr):
        return arr.reshape(seq_count, head_count, block_count, BLOCK, arr.shape[-1]).transpose(
            2, 0, 1, 3, 4
        )

    def advance(memory, inputs):
        q_block, k_block, v_block = inputs
        scores = jnp.einsum("shqd,shkd->shqk", q_block, k_block, preferred_element_type=jnp.float32)
        weights = (scores * inside).astype(jnp.bfloat16)
        within = jnp.einsum("shqk,shkv->shqv", weights, v_block, preferred_element_type=jnp.float32)
        carried = jnp.einsum("shqd,shdv->shqv", q_block.astype(jnp.float32) * query_scale, memory)
        k_scaled = (k_block.astype(jnp.float32) * key_scale).astype(jnp.bfloat16)
        memory = memory * block_decay + jnp.einsum(
            "shkd,shkv->shdv", k_scaled, v_block, preferred_element_type=jnp.float32
        )
        return (memory, within + carried)

    start_memory = jnp.zeros((seq_count, head_count, head_width, values.shape[-1]), jnp.float32)
    end_state, outputs = lax.scan(
        advance, start_memory, (to_blocks(queries), to_blocks(key_rows), to_blocks(values))
    )
    outputs = outputs.transpose(1, 2, 0, 3, 4).reshape(
        seq_count, head_count, length, values.shape[-1]
    )
    return (outputs, end_state)


def combine(earlier, later_part):
    return (
        earlier[0] * later_part[0],
        earlier[1] * later_part[0][None, :, None, None] + later_part[1],
    )


def read_out(carried, queries, partial_out, log_decay):
    length = queries.shape[2]
    read_scale = jnp.exp(log_decay[:, None] * (jnp.arange(length, dtype=jnp.float32) + 1.0))[
        ..., None
    ]
    return partial_out + jnp.einsum(
        "shld,shdv->shlv", queries.astype(jnp.float32) * read_scale, carried
    )


def body(
    tokens,
    in_gain,
    query_weight,
    key_weight,
    value_weight,
    gate_weight,
    log_decay,
    norm_gain,
    out_weight,
    post_gain,
):
    seq_count, rows_dev, model_width = tokens.shape
    tp_size = lax.axis_size("tp")
    local_width = query_weight.shape[1]
    head_count = local_width // HEAD_DIM
    stretch = rows_dev * tp_size
    tok_f32 = tokens.astype(jnp.float32)
    normed = (
        tok_f32 * lax.rsqrt(jnp.mean(tok_f32 * tok_f32, axis=-1, keepdims=True) + rms_eps) * in_gain
    ).astype(jnp.bfloat16)
    joined = jnp.concatenate([query_weight, key_weight, value_weight, gate_weight], axis=1)
    projected = jnp.einsum(
        "kux,xt->kut",
        lax.all_gather(normed, "tp", axis=1, tiled=True),
        joined,
        preferred_element_type=jnp.float32,
    ).astype(jnp.bfloat16)

    def heads_of(columns):
        return columns.reshape(seq_count, stretch, head_count, HEAD_DIM).transpose(0, 2, 1, 3)

    positions = lax.axis_index(SP) * stretch + jnp.arange(stretch, dtype=jnp.int32)
    queries = rotate(heads_of(projected[..., :local_width]), positions).astype(jnp.bfloat16)
    key_rows = (
        rotate(heads_of(projected[..., local_width : 2 * local_width]), positions)
        * HEAD_DIM ** (-0.5)
    ).astype(jnp.bfloat16)
    values = heads_of(projected[..., 2 * local_width : 3 * local_width])
    gating = projected[..., 3 * local_width :]
    partial_out, end_state = local_pass(queries, key_rows, values, log_decay)
    span_decay = jnp.exp(log_decay * stretch)
    carried = entering(
        (span_decay, end_state), SP, combine, (jnp.ones_like(span_decay), jnp.zeros_like(end_state))
    )[1]
    retained = read_out(carried, queries, partial_out, log_decay)
    center = jnp.mean(retained, axis=-1, keepdims=True)
    spread = jnp.mean(jnp.square(retained - center), axis=-1, keepdims=True)
    normal = (
        ((retained - center) * lax.rsqrt(spread + group_eps))
        .transpose(0, 2, 1, 3)
        .reshape(seq_count, stretch, local_width)
    )
    gated = (normal * norm_gain * jax.nn.silu(gating.astype(jnp.float32))).astype(jnp.bfloat16)
    premix = jnp.einsum(
        "hor,rn->hon",
        lax.all_to_all(gated, "tp", split_axis=1, concat_axis=2, tiled=True),
        out_weight,
        preferred_element_type=jnp.float32,
    )
    mixed = (
        premix * lax.rsqrt(jnp.mean(premix * premix, axis=-1, keepdims=True) + rms_eps) * post_gain
    )
    return mixed.astype(jnp.bfloat16)


def solution(mesh):
    torus = Mesh(mesh.devices.reshape(8, 4, mesh.shape["tp"]), ("sp_0", "sp_1", "tp"))
    return jax.shard_map(
        body,
        mesh=torus,
        in_specs=(
            P(None, SP_TP, None),
            P(),
            P(None, "tp"),
            P(None, "tp"),
            P(None, "tp"),
            P(None, "tp"),
            P("tp"),
            P("tp"),
            P(),
            P(),
        ),
        out_specs=P(None, SP_TP, None),
        check_vma=False,
    )
```

profile of v0, /device:TPU:1, one launch (start us, length us, event | category | flops | bytes accessed | tf_op | source)
XLA Modules:
  0.0 204.7 jit_solution(9332395953188734523)
XLA Ops:
  6.5 1.6 fusion.44
  8.1 2.6 %fusion.46 = bf16[4,64,2048]{2,1,0:T(8,128)(2,1)} fusion(bf16[4,64,2048]{2,1,0:T(8,128)(2,1)} %param.12, f32[2048]{0:T(1024)} %param.13, f32[4,64]{1,0:T(4,128)S(1)} %add_rsqrt_fusion.2), kind=kLoop, calls=%fused_computation.48 | loop fusion | flops 2097152 | bytes 2106368 | tf_op jit(solution)/shard_map/convert_element_type | solution.py:126
  10.9 0.2 copy.39
  11.1 0.2 copy.40
  11.3 0.5 copy-done.10
  11.8 0.2 copy.41
  12.0 0.2 copy.42
  13.0 0.5 multiply_cosine_fusion
  13.5 53.8 %all-gather.7.cloned.1.call-done = bf16[4,512,2048]{2,1,0:T(8,128)(2,1)} async-done(((bf16[4,64,2048]{2,1,0:T(8,128)(2,1)}), bf16[4,512,2048]{2,1,0:T(8,128)(2,1)}) %all-gather.7.cloned.1.call-update) | async-done | bytes 8388624 | tf_op jit(solution)/shard_map/all_gather | solution.py:130
  67.3 9.5 %fusion.54 = bf16[4,512,512]{1,2,0:T(8,128)(2,1)S(1)} fusion(bf16[4,512,2048]{2,1,0:T(8,128)(2,1)} %all-gather.7.cloned.1.call-done, bf16[2048,128]{0,1:T(8,128)(2,1)S(1)} %copy.42, bf16[2048,128]{0,1:T(8,128)(2,1)S(1)} %copy.41, bf16[2048,128]{0,1:T(8,128)(2,1)S(1)} %copy.40, bf16[2048,128]{0,1:T(8,128)(2,1)S(1)} %copy.39), kind=kOutput, calls=%fused_computation.59 | convolution fusion | flops 4304404480 | bytes 12582912 | tf_op jit(solution)/shard_map/kux,xt->kut/dot_general | solution.py:128
  76.9 1.0 slice_bitcast_fusion
  77.9 0.3 fusion.66
  78.4 0.3 copy.46
  78.8 0.3 copy-done.6
  79.3 0.3 copy.47
  79.8 0.3 copy.43
  80.3 1.3 copy.44
  81.6 1.2 reshape_transpose_reshape.3
  82.8 0.4 copy.45
  83.2 0.3 maximum_bitcast_fusion.4
  83.5 0.9 copy-done.1
  84.4 0.3 fusion.69
  84.8 11.9 %while.15 = (s32[]{:T(128)}, f32[4,1,128,128]{3,2,0,1:T(8,128)S(1)}, f32[4,4,1,128,128]{4,3,1,2,0:T(8,128)}, f32[1]{0:T(128)}, bf16[4,4,1,128,128]{4,3,1,2,0:T(8...) while((s32[]{:T(128)}, ...), condition=%wide.region_2.3_spmd.clone.clone.clone, body=%wide.region_1.2_spmd.clone.clone.clone.sunk | while | flops 67977728 | bytes 2496632 | solution.py:80
  84.8 0.7 select_bitcast_fusion.2
  85.5 0.3 fusion.146
  85.9 0.7 exponential_bitcast_fusion.3
  86.5 0.9 fusion.147
  87.5 0.3 fusion.145
  87.8 0.7 select_bitcast_fusion.2
  88.5 0.3 fusion.146
  88.8 0.7 exponential_bitcast_fusion.3
  89.5 0.9 fusion.147
  90.4 0.3 fusion.145
  90.8 0.7 select_bitcast_fusion.2
  91.5 0.3 fusion.146
  91.8 0.7 exponential_bitcast_fusion.3
  92.5 0.9 fusion.147
  93.4 0.3 fusion.145
  93.8 0.7 select_bitcast_fusion.2
  94.5 0.3 fusion.146
  94.8 0.7 exponential_bitcast_fusion.3
  95.5 0.9 fusion.147
  96.4 0.3 fusion.145
  96.8 0.7 copy-done
  97.5 0.6 dynamic-slice
  98.1 0.7 exponential_dynamic-update-slice_fusion
  98.8 8.4 %all-reduce = f32[4]{0:T(128)S(1)} all-reduce(f32[4]{0:T(128)S(1)} %exponential_dynamic-update-slice_fusion), channel_id=2, replica_groups=mesh['sp_0'=8,'sp_1'=4,'tp'=8] {'sp_1'}, use_global_device_ids=true, to_apply=%add | all-reduce | flops 4 | bytes 32
  107.2 0.7 slice_multiply_fusion.1
  107.9 1.3 slice_multiply_fusion
  109.9 12.2 %all-gather.11.cloned.1.call-done = f32[16,1,128,128]{3,2,1,0:T(8,128)} async-done(((f32[4,1,128,128]{3,2,1,0:T(8,128)}), f32[16,1,128,128]{3,2,1,0:T(8,128)}) %all-gather.11.cloned.1.call-update) | async-done | bytes 1048592 | tf_op jit(solution)/shard_map/all_gather | solution.py:27
  122.0 3.8 %slice_add_fusion.8 = f32[4,1,128,128]{3,2,1,0:T(8,128)} fusion(f32[16,1,128,128]{3,2,1,0:T(8,128)} %all-gather.11.cloned.1.call-done, f32[]{:T(128)} %bitcast.20, f32[]{:T(128)} %bitcast.18, f32[16,1,128,128]{3,2,0,1:T(8,128)} %bitcast.197, f32[]{:T(128)} %bitcast.16, f32[]{:T(128)} %bitcast.13), kind=kLoop, calls=%fused_computation.109 | loop fusion | flops 458752 | bytes 1310736 | tf_op jit(solution)/shard_map/add | solution.py:92
  125.9 0.6 dynamic-slice.1
  126.4 1.3 dynamic-update-slice.1
  127.7 13.9 %all-reduce.1 = f32[8]{0:T(128)S(1)} all-reduce(f32[8]{0:T(128)S(1)} %dynamic-update-slice.1), channel_id=3, replica_groups=mesh['sp_0'=8,'sp_1'=4,'tp'=8] {'sp_0'}, use_global_device_ids=true, to_apply=%add.1 | all-reduce | flops 8 | bytes 64
  141.6 0.7 fusion.127
  145.5 0.4 copy.48
  145.9 0.4 reshape.499
  146.3 18.7 %all-gather.9.cloned.1.call-done = f32[8,4,1,128,128]{4,3,2,1,0:T(8,128)} async-done(((f32[1,4,1,128,128]{4,3,2,1,0:T(8,128)}), f32[8,4,1,128,128]{4,3,2,1,0:T(8,128)}) %all-gather.9.cloned.1.call-update) | async-done | bytes 2097168 | tf_op jit(solution)/shard_map/all_gather | solution.py:27
  165.1 7.9 %fusion.128 = (f32[4,512]{1,0:T(4,128)S(1)}, f32[4,512,128]{1,2,0:T(8,128)S(1)}) fusion(f32[4,512,128]{1,2,0:T(8,128)S(1)} %reshape.499, f32[8,4,1,128,128]{4,3,1,2,0:T(8,128)} %bitcast.204, f32[4,1,128,128]{3,2,1,0:T(8,128)S(1)} %copy-done.4, f32[16,1,128,128]{3,2,0,1:T(8,128)S(1)} %bitcast.198, f32[16,1,128,128]{3,2,1,0:T(8,128)S(1)} %copy-done.3, ...), kind=kOutput, calls=%fused_computation.175 | convolution fusion | flops 71170048 | bytes 5777468 | tf_op jit(solution)/shard_map/shld,shdv->shlv/dot_general | solution.py:101
  173.2 1.5 fusion.62
  174.7 0.3 copy.65
  175.0 18.3 %all_to_all.18 = bf16[4,512,128]{2,0,1:T(4,128)(2,1)S(1)} all-to-all(bf16[4,512,128]{2,0,1:T(4,128)(2,1)S(1)} %copy.65), channel_id=1, replica_groups=mesh['sp_0'=8,'sp_1'=4,'tp'=8] {'tp'}, dimensions={1} | all-to-all | bytes 1048576 | tf_op jit(solution)/shard_map/all_to_all | solution.py:162
  193.4 3.6 %multiply_reduce_fusion = (f32[4,64]{1,0:T(4,128)S(1)}, f32[4,64,2048]{2,1,0:T(8,128)S(1)}) fusion(bf16[1024,2048]{1,0:T(8,128)(2,1)} %param.20, bf16[4,8,8,8,128]{4,3,2,1,0:T(8,128)(2,1)S(1)} %bitcast.203), kind=kOutput, calls=%fused_computation.58 | convolution fusion | flops 1074790144 | bytes 6816768 | tf_op jit(solution)/shard_map/hor,rn->hon/dot_general | solution.py:160
  197.0 1.2 multiply_convert_fusion.2
  (51 shorter events, 1.3 us)
Async XLA Ops:
  6.5 4.3 %copy-start.8 = (bf16[2048,128]{1,0:T(8,128)(2,1)S(1)}, bf16[2048,128]{1,0:T(8,128)(2,1)}, u32[]{:S(2)}) copy-start(bf16[2048,128]{1,0:T(8,128)(2,1)} %param.14) | copy-start | bytes 1572868
  6.5 60.8 %all-gather.7.cloned.1.call-start = ((), (), s32[]{:S(2)}) async-start(), calls=%async_computation.1 | async-start | bytes 9437184 | tf_op jit(solution)/shard_map/all_gather | solution.py:130
  8.1 3.0 %copy-start.9 = (bf16[2048,128]{1,0:T(8,128)(2,1)S(1)}, bf16[2048,128]{1,0:T(8,128)(2,1)}, u32[]{:S(2)}) copy-start(bf16[2048,128]{1,0:T(8,128)(2,1)} %param.15) | copy-start | bytes 1572868
  10.8 1.0 copy-start.10
  10.8 1.3 copy-start.11
  10.8 111.2 %all-gather.11.cloned.1.call-start = ((), (), s32[]{:S(2)}) async-start(), calls=%async_computation.3 | async-start | bytes 1310720 | tf_op jit(solution)/shard_map/all_gather | solution.py:27
  76.9 1.5 copy-start.2
  78.3 0.7 copy-start.6
  78.4 0.8 copy-start.7
  83.2 1.2 copy-start.1
  84.8 12.8 %copy-start.15 = (u32[256]{0:T(256)S(1)}, u32[256]{0:T(256)}, u32[]{:S(2)}) copy-start(u32[256]{0:T(256)} %constant.86) | copy-start | bytes 3076
  84.8 41.1 %copy-start.14 = (u32[256]{0:T(256)S(1)}, u32[256]{0:T(256)}, u32[]{:S(2)}) copy-start(u32[256]{0:T(256)} %constant.91) | copy-start | bytes 3076
  96.7 0.7 copy-start
  96.7 48.7 %copy-start.5 = (f32[4,4,1,128,128]{4,3,1,2,0:T(8,128)S(1)}, f32[4,4,1,128,128]{4,3,1,2,0:T(8,128)}, u32[]{:S(2)}) copy-start(f32[4,4,1,128,128]{4,3,1,2,0:T(8,128)} %get-tuple-element.58) | copy-start | bytes 3145732
  97.5 67.6 %all-gather.9.cloned.1.call-start = ((), (), s32[]{:S(2)}) async-start(), calls=%async_computation.2 | async-start | bytes 2359296 | tf_op jit(solution)/shard_map/all_gather | solution.py:27
  145.5 19.6 %copy-start.3 = (f32[16,1,128,128]{3,2,1,0:T(8,128)S(1)}, f32[16,1,128,128]{3,2,1,0:T(8,128)}, u32[]{:S(2)}) copy-start(f32[16,1,128,128]{3,2,1,0:T(8,128)} %all-gather.11.cloned.1.call-done) | copy-start | bytes 3145732
  145.5 19.6 %copy-start.4 = (f32[4,1,128,128]{3,2,1,0:T(8,128)S(1)}, f32[4,1,128,128]{3,2,1,0:T(8,128)}, u32[]{:S(2)}) copy-start(f32[4,1,128,128]{3,2,1,0:T(8,128)} %slice_add_fusion.8) | copy-start | bytes 786436
  165.1 8.1 %copy-start.13 = (f32[128]{0:T(128)S(1)}, f32[128]{0:T(128)}, u32[]{:S(2)}) copy-start(f32[128]{0:T(128)} %param.19) | copy-start | bytes 1540
  193.4 3.6 %copy-start.12 = (f32[2048]{0:T(1024)S(1)}, f32[2048]{0:T(1024)}, u32[]{:S(2)}) copy-start(f32[2048]{0:T(1024)} %param.21) | copy-start | bytes 24580
Sparse Core Ops, SparseCore 0:
  10.9 56.3 all-gather.6
  97.6 24.3 all-gather.10
  126.0 39.0 all-gather.8
where the time goes:
time: 205 us
  waiting for transfers between devices  84.8 us (41%)
  blocking collectives  40.6 us (20%)
  matrix products  27.4 us (13%)
  other arithmetic  20.4 us (10%)
  between operations  18 us (9%)
  local copies, waits for them, and re-layouts  13.3 us (6%)
    all_gather x1, waiting for transfers between devices, body(): lax.all_gather(normed, 'tp', axis=1, tiled=True)  53.8 us
    all_gather x2, waiting for transfers between devices, entering(): pieces = jax.tree.map(lambda part: lax.all_gather(part, axis), running)  30.9 us
    unnamed x2, blocking collectives  22.3 us
    all_to_all x1, blocking collectives, body(): lax.all_to_all(gated, 'tp', split_axis=1, concat_axis=2, tiled=True)  18.3 us
    dot_general x1, matrix products, body(): jnp.einsum('kux,xt->kut', lax.all_gather(normed, 'tp', axis=1, tiled=True...  9.51 us
    dot_general x1, matrix products, read_out(): jnp.einsum('shld,shdv->shlv', queries.astype(jnp.float32) * read_scale, c...  7.93 us
    unnamed x41, local copies, waits for them, and re-layouts  6.03 us
  transfers between devices with their start and end apart: 3, of which 3 were waited for; matrix products, arithmetic and copies ran while one was open for 4% of the time, Pallas kernels for 0%

commit v1 on v0

--- a/solution.py
+++ b/solution.py
@@ -115,6 +115,31 @@
     out_weight,
     post_gain,
 ):
+
+    def get_quotas_on_mesh(x_local, ax_name):
+        val = lax.psum(1, ax_name)
+        w_next = lax.axis_index(ax_name)
+        right_arr, upper, even = (val, w_next, x_local.shape[1])
+        blocks_here = tuple(((h, (h + 1) % right_arr) for h in range(right_arr)))
+        ledger = tuple(((h, (h - 1) % right_arr) for h in range(right_arr)))
+        oldest = jnp.zeros(
+            (*x_local.shape[:1], right_arr * even, *x_local.shape[2:]), x_local.dtype
+        )
+        oldest = lax.dynamic_update_slice_in_dim(oldest, x_local, upper * even, axis=1)
+        current_arr = tmp = x_local
+        item_now = right_arr // 2
+        for pp in range(1, item_now + 1):
+            current_arr = lax.ppermute(current_arr, ax_name, blocks_here)
+            oldest = lax.dynamic_update_slice_in_dim(
+                oldest, current_arr, (upper - pp) % right_arr * even, axis=1
+            )
+            if pp < right_arr - item_now:
+                tmp = lax.ppermute(tmp, ax_name, ledger)
+                oldest = lax.dynamic_update_slice_in_dim(
+                    oldest, tmp, (upper + pp) % right_arr * even, axis=1
+                )
+        return oldest
+
     seq_count, rows_dev, model_width = tokens.shape
     tp_size = lax.axis_size("tp")
     local_width = query_weight.shape[1]
@@ -126,10 +151,7 @@
     ).astype(jnp.bfloat16)
     joined = jnp.concatenate([query_weight, key_weight, value_weight, gate_weight], axis=1)
     projected = jnp.einsum(
-        "kux,xt->kut",
-        lax.all_gather(normed, "tp", axis=1, tiled=True),
-        joined,
-        preferred_element_type=jnp.float32,
+        "kux,xt->kut", get_quotas_on_mesh(normed, "tp"), joined, preferred_element_type=jnp.float32
     ).astype(jnp.bfloat16)
 
     def heads_of(columns):

time: 205 us -> 219 us (1.068)
  waiting for transfers between devices: 84.8 us -> 62 us
  local copies, waits for them, and re-layouts: 13.3 us -> 36 us
  starting transfers between devices: 0.09 us -> 12.8 us
    all_gather x1 -> x0, waiting for transfers between devices: 53.8 us -> none  [body(): lax.all_gather(normed, 'tp', axis=1, tiled=True)]
    ppermute x0 -> x7, waiting for transfers between devices: none -> 26.9 us  [the longest x4 23 us: get_quotas_on_mesh(): current_arr = lax.ppermute(current_arr, ax_name, blocks_here)]
    ppermute x0 -> x7, starting transfers between devices: none -> 12.7 us  [the longest x4 7.69 us: get_quotas_on_mesh(): current_arr = lax.ppermute(current_arr, ax_name, blocks_here)]
    dynamic_update_slice x0 -> x7, local copies, waits for them, and re-layouts: none -> 9.89 us  [the longest x4 6.75 us: get_quotas_on_mesh(): lax.dynamic_update_slice_in_dim(oldest, current_arr, (upper - pp) % right...]
    unnamed x41, local copies, waits for them, and re-layouts: 6.03 us -> 13.4 us
    broadcast_in_dim x0 -> x1, local copies, waits for them, and re-layouts: none -> 4.32 us  [get_quotas_on_mesh(): jnp.zeros((*x_local.shape[:1], right_arr * even, *x_local.shape[2:]), x_l...]
    all_gather x2, waiting for transfers between devices: 30.9 us -> 35.1 us  [entering(): pieces = jax.tree.map(lambda part: lax.all_gather(part, axis), running)]
    convert_element_type x1 -> x0, other arithmetic: 2.65 us -> none  [body(): normed = (tok_f32 * lax.rsqrt(jnp.mean(tok_f32 * tok_f32, axis=-1, keepdi...]
  transfers between devices with their start and end apart: 3 -> 9, of which waited for: 3 -> 7; matrix products, arithmetic and copies ran while one was open for 4% -> 12% of each run, Pallas kernels for 0% -> 0%
where the time goes in v1:
time: 219 us; the launch traced here: 218 us
  waiting for transfers between devices  62 us (28%)
  blocking collectives  40.7 us (19%)
  local copies, waits for them, and re-layouts  36 us (16%)
  matrix products  27.4 us (13%)
  other arithmetic  20.3 us (9%)
  between operations  18.3 us (8%)
  starting transfers between devices  12.8 us (6%)
    all_gather x2, waiting for transfers between devices, entering(): pieces = jax.tree.map(lambda part: lax.all_gather(part, axis), running)  35.1 us
    ppermute x4, waiting for transfers between devices, get_quotas_on_mesh(): current_arr = lax.ppermute(current_arr, ax_name, blocks_here)  23 us
    unnamed x2, blocking collectives  22.2 us
    all_to_all x1, blocking collectives, body(): lax.all_to_all(gated, 'tp', split_axis=1, concat_axis=2, tiled=True)  18.6 us
    unnamed x41, local copies, waits for them, and re-layouts  13.4 us
    dot_general x1, matrix products, body(): jnp.einsum('kux,xt->kut', get_quotas_on_mesh(normed, 'tp'), joined, prefe...  9.66 us
    dot_general x1, matrix products, read_out(): jnp.einsum('shld,shdv->shlv', queries.astype(jnp.float32) * read_scale, c...  7.81 us
    ppermute x4, starting transfers between devices, get_quotas_on_mesh(): current_arr = lax.ppermute(current_arr, ax_name, blocks_here)  7.69 us
  transfers between devices with their start and end apart: 9, of which 7 were waited for; matrix products, arithmetic and copies ran while one was open for 12% of the time, Pallas kernels for 0%

profile of v1, /device:TPU:1, one launch (start us, length us, event | category | flops | bytes accessed | tf_op | source)
XLA Modules:
  0.0 217.7 jit_solution(1565288610632173341)
XLA Ops:
  6.5 1.5 fusion.44
  8.1 4.3 %broadcast_in_dim.10 = bf16[4,512,2048]{2,1,0:T(8,128)(2,1)} broadcast(bf16[]{:T(256)} %constant.98.clone.1), dimensions={} | broadcast | bytes 8388610 | tf_op jit(solution)/shard_map/broadcast_in_dim | solution.py:125
  12.4 1.3 constant_dynamic-update-slice_fusion.7
  13.7 2.6 %collective-permute-start = (bf16[4,64,2048]{2,1,0:T(8,128)(2,1)S(1)}, bf16[4,64,2048]{2,1,0:T(8,128)(2,1)}, u32[]{:S(2)}, u32[]{:S(2)}) collective-permute-start(bf16[4,64,2048]{2,1,0:T(8,128)(2,1)S(1)} %get-tuple-element.162), channel_id=1, source_target_pairs={{0,1},{1,2},{2,3},{3,4},{4,5},{5,6},{6,7},{7,0},{8,9},{9,10},{10,1... | collective-permute-start | bytes 3145736 | tf_op jit(solution)/shard_map/ppermute | solution.py:132
  16.3 0.6 collective-permute-start.1
  16.9 11.2 %collective-permute-done = bf16[4,64,2048]{2,1,0:T(8,128)(2,1)} collective-permute-done((bf16[4,64,2048]{2,1,0:T(8,128)(2,1)S(1)}, bf16[4,64,2048]{2,1,0:T(8,128)(2,1)}, u32[]{:S(2)}, u32[]{:S(2)}) %collective-permute-start) | collective-permute-done | bytes 1048608 | tf_op jit(solution)/shard_map/ppermute | solution.py:132
  28.1 2.6 %collective-permute-start.2 = (bf16[4,64,2048]{2,1,0:T(8,128)(2,1)}, bf16[4,64,2048]{2,1,0:T(8,128)(2,1)}, u32[]{:S(2)}, u32[]{:S(2)}) collective-permute-start(bf16[4,64,2048]{2,1,0:T(8,128)(2,1)} %collective-permute-done), channel_id=1, source_target_pairs={{0,1},{1,2},{2,3},{3,4},{4,5},{5,6},{6,7},{7,0},{8,9},{9,10},{10,1... | collective-permute-start | bytes 3145736 | tf_op jit(solution)/shard_map/ppermute | solution.py:132
  30.9 1.5 collective-permute-start.3
  32.4 10.3 %collective-permute-done.2 = bf16[4,64,2048]{2,1,0:T(8,128)(2,1)} collective-permute-done((bf16[4,64,2048]{2,1,0:T(8,128)(2,1)}, bf16[4,64,2048]{2,1,0:T(8,128)(2,1)}, u32[]{:S(2)}, u32[]{:S(2)}) %collective-permute-start.2) | collective-permute-done | bytes 1048608 | tf_op jit(solution)/shard_map/ppermute | solution.py:132
  42.7 2.5 %collective-permute-start.4 = (bf16[4,64,2048]{2,1,0:T(8,128)(2,1)}, bf16[4,64,2048]{2,1,0:T(8,128)(2,1)S(1)}, u32[]{:S(2)}, u32[]{:S(2)}) collective-permute-start(bf16[4,64,2048]{2,1,0:T(8,128)(2,1)} %collective-permute-done.2), channel_id=1, source_target_pairs={{0,1},{1,2},{2,3},{3,4},{4,5},{5,6},{6,7},{7,0},{8,9},{9,10},{10,1... | collective-permute-start | bytes 3145736 | tf_op jit(solution)/shard_map/ppermute | solution.py:132
  45.2 2.1 copy.39
  47.3 2.0 copy.40
  49.3 2.0 copy.41
  51.4 2.0 copy.42
  54.2 0.5 multiply_cosine_fusion
  54.7 3.0 %collective-permute-start.5 = (bf16[4,64,2048]{2,1,0:T(8,128)(2,1)S(1)}, bf16[4,64,2048]{2,1,0:T(8,128)(2,1)S(1)}, u32[]{:S(2)}, u32[]{:S(2)}) collective-permute-start(bf16[4,64,2048]{2,1,0:T(8,128)(2,1)S(1)} %collective-permute-done.3), channel_id=1, source_target_pairs={{0,7},{1,0},{2,1},{3,2},{4,3},{5,4},{6,5},{7,6},{8,15},{9,8},{10,9... | collective-permute-start | bytes 3145736 | tf_op jit(solution)/shard_map/ppermute | solution.py:137
  57.7 2.3 %constant_dynamic-update-slice_fusion.6 = bf16[4,512,2048]{2,1,0:T(8,128)(2,1)} fusion(bf16[4,512,2048]{2,1,0:T(8,128)(2,1)} %get-tuple-element.161, bf16[4,64,2048]{2,1,0:T(8,128)(2,1)} %collective-permute-done, s32[]{:T(128)S(6)} %select_n.213), kind=kLoop, calls=%fused_computation.172 | loop fusion | bytes 2097156 | tf_op jit(solution)/shard_map/dynamic_update_slice | solution.py:133
  60.0 1.1 constant_dynamic-update-slice_fusion.5
  61.1 2.4 %constant_dynamic-update-slice_fusion.4 = bf16[4,512,2048]{2,1,0:T(8,128)(2,1)} fusion(bf16[4,512,2048]{2,1,0:T(8,128)(2,1)} %constant_dynamic-update-slice_fusion.5, bf16[4,64,2048]{2,1,0:T(8,128)(2,1)} %collective-permute-done.2, s32[]{:T(128)S(6)} %select_n.217), kind=kLoop, calls=%fused_computation.170 | loop fusion | bytes 2097156 | tf_op jit(solution)/shard_map/dynamic_update_slice | solution.py:133
  63.5 1.0 constant_dynamic-update-slice_fusion.3
  64.5 1.1 constant_dynamic-update-slice_fusion.2
  65.6 3.7 %collective-permute-done.5 = bf16[4,64,2048]{2,1,0:T(8,128)(2,1)S(1)} collective-permute-done((bf16[4,64,2048]{2,1,0:T(8,128)(2,1)S(1)}, bf16[4,64,2048]{2,1,0:T(8,128)(2,1)S(1)}, u32[]{:S(2)}, u32[]{:S(2)}) %collective-permute-start.5) | collective-permute-done | bytes 1048608 | tf_op jit(solution)/shard_map/ppermute | solution.py:137
  69.2 1.0 constant_dynamic-update-slice_fusion.1
  70.3 1.5 collective-permute-done.6
  71.8 1.0 constant_dynamic-update-slice_fusion
  72.8 9.7 %fusion.54 = bf16[4,512,512]{1,2,0:T(8,128)(2,1)S(1)} fusion(bf16[4,512,2048]{2,1,0:T(8,128)(2,1)} %constant_dynamic-update-slice_fusion, bf16[2048,128]{0,1:T(8,128)(2,1)S(1)} %copy-done.10, bf16[2048,128]{0,1:T(8,128)(2,1)S(1)} %copy-done.9, bf16[2048,128]{0,1:T(8,128)(2,1)S(1)} %copy-done.8, bf16[2048,128]{0,1:T(8,128)(2,1)S(1)} %copy-done.7), kind=kOutput, calls=%fused_computation.59 | convolution fusion | flops 4304404480 | bytes 12582912 | tf_op jit(solution)/shard_map/kux,xt->kut/dot_general | solution.py:153
  82.5 1.3 copy-done.2
  83.8 0.9 slice_bitcast_fusion
  87.0 1.3 copy.44
  88.3 1.2 reshape_transpose_reshape.3
  90.2 1.6 fusion.69
  91.8 11.9 %while.15 = (s32[]{:T(128)}, f32[4,1,128,128]{3,2,0,1:T(8,128)S(1)}, f32[4,4,1,128,128]{4,3,1,2,0:T(8,128)}, f32[1]{0:T(128)}, bf16[4,4,1,128,128]{4,3,1,2,0:T(8...) while((s32[]{:T(128)}, ...), condition=%wide.region_2.3_spmd.clone.clone.clone, body=%wide.region_1.2_spmd.clone.clone.clone.sunk | while | flops 67977728 | bytes 2496632 | solution.py:80
  91.8 0.7 select_bitcast_fusion.2
  92.8 0.7 exponential_bitcast_fusion.3
  93.5 0.9 fusion.148
  94.8 0.7 select_bitcast_fusion.2
  95.8 0.7 exponential_bitcast_fusion.3
  96.5 0.9 fusion.148
  97.7 0.7 select_bitcast_fusion.2
  98.8 0.7 exponential_bitcast_fusion.3
  99.4 0.9 fusion.148
  100.7 0.7 select_bitcast_fusion.2
  101.8 0.7 exponential_bitcast_fusion.3
  102.4 0.9 fusion.148
  103.7 0.7 copy-done
  104.5 0.7 dynamic-slice
  105.2 0.8 exponential_dynamic-update-slice_fusion
  106.0 8.3 %all-reduce = f32[4]{0:T(128)S(1)} all-reduce(f32[4]{0:T(128)S(1)} %exponential_dynamic-update-slice_fusion), channel_id=2, replica_groups=mesh['sp_0'=8,'sp_1'=4,'tp'=8] {'sp_1'}, use_global_device_ids=true, to_apply=%add | all-reduce | flops 4 | bytes 32
  114.2 0.6 slice_multiply_fusion.1
  114.9 1.3 slice_multiply_fusion
  116.8 18.0 %all-gather.8.cloned.1.call-done = f32[16,1,128,128]{3,2,1,0:T(8,128)} async-done(((f32[4,1,128,128]{3,2,1,0:T(8,128)}), f32[16,1,128,128]{3,2,1,0:T(8,128)}) %all-gather.8.cloned.1.call-update) | async-done | bytes 1048592 | tf_op jit(solution)/shard_map/all_gather | solution.py:27
  134.8 3.8 %slice_add_fusion.8 = f32[4,1,128,128]{3,2,1,0:T(8,128)} fusion(f32[16,1,128,128]{3,2,1,0:T(8,128)} %all-gather.8.cloned.1.call-done, f32[]{:T(128)} %bitcast.20, f32[]{:T(128)} %bitcast.18, f32[16,1,128,128]{3,2,0,1:T(8,128)} %bitcast.197, f32[]{:T(128)} %bitcast.16, f32[]{:T(128)} %bitcast.13), kind=kLoop, calls=%fused_computation.109 | loop fusion | flops 458752 | bytes 1310736 | tf_op jit(solution)/shard_map/add | solution.py:92
  138.7 0.7 dynamic-slice.1
  139.3 1.4 dynamic-update-slice.1
  140.7 13.9 %all-reduce.1 = f32[8]{0:T(128)S(1)} all-reduce(f32[8]{0:T(128)S(1)} %dynamic-update-slice.1), channel_id=3, replica_groups=mesh['sp_0'=8,'sp_1'=4,'tp'=8] {'sp_0'}, use_global_device_ids=true, to_apply=%add.1 | all-reduce | flops 8 | bytes 64
  154.6 0.7 fusion.128
  158.4 1.6 copy.48
  160.1 0.4 reshape.499
  160.5 17.1 %all-gather.6.cloned.1.call-done = f32[8,4,1,128,128]{4,3,2,1,0:T(8,128)} async-done(((f32[1,4,1,128,128]{4,3,2,1,0:T(8,128)}), f32[8,4,1,128,128]{4,3,2,1,0:T(8,128)}) %all-gather.6.cloned.1.call-update) | async-done | bytes 2097168 | tf_op jit(solution)/shard_map/all_gather | solution.py:27
  177.6 7.8 %fusion.129 = (f32[4,512]{1,0:T(4,128)S(1)}, f32[4,512,128]{1,2,0:T(8,128)S(1)}) fusion(f32[4,512,128]{1,2,0:T(8,128)S(1)} %reshape.499, f32[8,4,1,128,128]{4,3,1,2,0:T(8,128)} %bitcast.204, f32[4,1,128,128]{3,2,1,0:T(8,128)S(1)} %copy-done.4, f32[16,1,128,128]{3,2,0,1:T(8,128)S(1)} %bitcast.198, f32[16,1,128,128]{3,2,1,0:T(8,128)S(1)} %copy-done.3, ...), kind=kOutput, calls=%fused_computation.183 | convolution fusion | flops 71170048 | bytes 5777468 | tf_op jit(solution)/shard_map/shld,shdv->shlv/dot_general | solution.py:101
  185.6 1.5 fusion.62
  187.4 18.6 %all_to_all.18 = bf16[4,512,128]{2,0,1:T(4,128)(2,1)S(1)} all-to-all(bf16[4,512,128]{2,0,1:T(4,128)(2,1)S(1)} %copy.65), channel_id=1, replica_groups=mesh['sp_0'=8,'sp_1'=4,'tp'=8] {'tp'}, dimensions={1} | all-to-all | bytes 1048576 | tf_op jit(solution)/shard_map/all_to_all | solution.py:184
  206.1 3.6 %multiply_reduce_fusion = (f32[4,64]{1,0:T(4,128)S(1)}, f32[4,64,2048]{2,1,0:T(8,128)S(1)}) fusion(bf16[1024,2048]{1,0:T(8,128)(2,1)} %param.20, bf16[4,8,8,8,128]{4,3,2,1,0:T(8,128)(2,1)S(1)} %bitcast.203), kind=kOutput, calls=%fused_computation.58 | convolution fusion | flops 1074790144 | bytes 6816768 | tf_op jit(solution)/shard_map/hor,rn->hon/dot_general | solution.py:182
  209.6 1.2 multiply_convert_fusion.2
  (70 shorter events, 6.5 us)
Async XLA Ops:
  6.5 128.2 %all-gather.8.cloned.1.call-start = ((), (), s32[]{:S(2)}) async-start(), calls=%async_computation.2 | async-start | bytes 1310720 | tf_op jit(solution)/shard_map/all_gather | solution.py:27
  8.1 4.3 %copy-start.1 = (bf16[4,64,2048]{2,1,0:T(8,128)(2,1)S(1)}, bf16[4,64,2048]{2,1,0:T(8,128)(2,1)}, u32[]{:S(2)}) copy-start(bf16[4,64,2048]{2,1,0:T(8,128)(2,1)} %param.12) | copy-start | bytes 3145732
  8.1 4.3 %copy-start.11 = (f32[2048]{0:T(1024)S(1)}, f32[2048]{0:T(1024)}, u32[]{:S(2)}) copy-start(f32[2048]{0:T(1024)} %param.13) | copy-start | bytes 24580
  13.7 14.4 %collective-permute-start = (bf16[4,64,2048]{2,1,0:T(8,128)(2,1)S(1)}, bf16[4,64,2048]{2,1,0:T(8,128)(2,1)}, u32[]{:S(2)}, u32[]{:S(2)}) collective-permute-start(bf16[4,64,2048]{2,1,0:T(8,128)(2,1)S(1)} %get-tuple-element.162), channel_id=1, source_target_pairs={{0,1},{1,2},{2,3},{3,4},{4,5},{5,6},{6,7},{7,0},{8,9},{9,10},{10,1... | collective-permute-start | bytes 3145736 | tf_op jit(solution)/shard_map/ppermute | solution.py:132
  16.3 14.6 %collective-permute-start.1 = (bf16[4,64,2048]{2,1,0:T(8,128)(2,1)S(1)}, bf16[4,64,2048]{2,1,0:T(8,128)(2,1)S(1)}, u32[]{:S(2)}, u32[]{:S(2)}) collective-permute-start(bf16[4,64,2048]{2,1,0:T(8,128)(2,1)S(1)} %get-tuple-element.162), channel_id=1, source_target_pairs={{0,7},{1,0},{2,1},{3,2},{4,3},{5,4},{6,5},{7,6},{8,15},{9,8},{10,9... | collective-permute-start | bytes 3145736 | tf_op jit(solution)/shard_map/ppermute | solution.py:137
  28.1 14.6 %collective-permute-start.2 = (bf16[4,64,2048]{2,1,0:T(8,128)(2,1)}, bf16[4,64,2048]{2,1,0:T(8,128)(2,1)}, u32[]{:S(2)}, u32[]{:S(2)}) collective-permute-start(bf16[4,64,2048]{2,1,0:T(8,128)(2,1)} %collective-permute-done), channel_id=1, source_target_pairs={{0,1},{1,2},{2,3},{3,4},{4,5},{5,6},{6,7},{7,0},{8,9},{9,10},{10,1... | collective-permute-start | bytes 3145736 | tf_op jit(solution)/shard_map/ppermute | solution.py:132
  30.9 23.8 %collective-permute-start.3 = (bf16[4,64,2048]{2,1,0:T(8,128)(2,1)S(1)}, bf16[4,64,2048]{2,1,0:T(8,128)(2,1)S(1)}, u32[]{:S(2)}, u32[]{:S(2)}) collective-permute-start(bf16[4,64,2048]{2,1,0:T(8,128)(2,1)S(1)} %collective-permute-done.1), channel_id=1, source_target_pairs={{0,7},{1,0},{2,1},{3,2},{4,3},{5,4},{6,5},{7,6},{8,15},{9,8},{10,9... | collective-permute-start | bytes 3145736 | tf_op jit(solution)/shard_map/ppermute | solution.py:137
  42.7 17.3 %collective-permute-start.4 = (bf16[4,64,2048]{2,1,0:T(8,128)(2,1)}, bf16[4,64,2048]{2,1,0:T(8,128)(2,1)S(1)}, u32[]{:S(2)}, u32[]{:S(2)}) collective-permute-start(bf16[4,64,2048]{2,1,0:T(8,128)(2,1)} %collective-permute-done.2), channel_id=1, source_target_pairs={{0,1},{1,2},{2,3},{3,4},{4,5},{5,6},{6,7},{7,0},{8,9},{9,10},{10,1... | collective-permute-start | bytes 3145736 | tf_op jit(solution)/shard_map/ppermute | solution.py:132
  54.7 14.5 %collective-permute-start.5 = (bf16[4,64,2048]{2,1,0:T(8,128)(2,1)S(1)}, bf16[4,64,2048]{2,1,0:T(8,128)(2,1)S(1)}, u32[]{:S(2)}, u32[]{:S(2)}) collective-permute-start(bf16[4,64,2048]{2,1,0:T(8,128)(2,1)S(1)} %collective-permute-done.3), channel_id=1, source_target_pairs={{0,7},{1,0},{2,1},{3,2},{4,3},{5,4},{6,5},{7,6},{8,15},{9,8},{10,9... | collective-permute-start | bytes 3145736 | tf_op jit(solution)/shard_map/ppermute | solution.py:137
  60.0 11.7 %collective-permute-start.6 = (bf16[4,64,2048]{2,1,0:T(8,128)(2,1)S(1)}, bf16[4,64,2048]{2,1,0:T(8,128)(2,1)S(1)}, u32[]{:S(2)}, u32[]{:S(2)}) collective-permute-start(bf16[4,64,2048]{2,1,0:T(8,128)(2,1)S(1)} %collective-permute-done.4), channel_id=1, source_target_pairs={{0,1},{1,2},{2,3},{3,4},{4,5},{5,6},{6,7},{7,0},{8,9},{9,10},{10,1... | collective-permute-start | bytes 3145736 | tf_op jit(solution)/shard_map/ppermute | solution.py:132
  63.4 9.4 %copy-start.7 = (bf16[2048,128]{0,1:T(8,128)(2,1)S(1)}, bf16[2048,128]{0,1:T(8,128)(2,1)}, u32[]{:S(2)}) copy-start(bf16[2048,128]{0,1:T(8,128)(2,1)} %copy.39) | copy-start | bytes 1572868
  63.4 9.4 %copy-start.8 = (bf16[2048,128]{0,1:T(8,128)(2,1)S(1)}, bf16[2048,128]{0,1:T(8,128)(2,1)}, u32[]{:S(2)}) copy-start(bf16[2048,128]{0,1:T(8,128)(2,1)} %copy.40) | copy-start | bytes 1572868
  63.5 9.4 %copy-start.9 = (bf16[2048,128]{0,1:T(8,128)(2,1)S(1)}, bf16[2048,128]{0,1:T(8,128)(2,1)}, u32[]{:S(2)}) copy-start(bf16[2048,128]{0,1:T(8,128)(2,1)} %copy.41) | copy-start | bytes 1572868
  63.5 9.4 %copy-start.10 = (bf16[2048,128]{0,1:T(8,128)(2,1)S(1)}, bf16[2048,128]{0,1:T(8,128)(2,1)}, u32[]{:S(2)}) copy-start(bf16[2048,128]{0,1:T(8,128)(2,1)} %copy.42) | copy-start | bytes 1572868
  82.5 1.3 copy-start.2
  85.0 0.7 copy-start.5
  85.0 0.8 copy-start.6
  91.7 12.8 %copy-start.15 = (u32[256]{0:T(256)S(1)}, u32[256]{0:T(256)}, u32[]{:S(2)}) copy-start(u32[256]{0:T(256)} %constant.135) | copy-start | bytes 3076
  91.8 46.9 %copy-start.14 = (u32[256]{0:T(256)S(1)}, u32[256]{0:T(256)}, u32[]{:S(2)}) copy-start(u32[256]{0:T(256)} %constant.140) | copy-start | bytes 3076
  103.7 0.7 copy-start
  104.4 73.2 %all-gather.6.cloned.1.call-start = ((), (), s32[]{:S(2)}) async-start(), calls=%async_computation.1 | async-start | bytes 2359296 | tf_op jit(solution)/shard_map/all_gather | solution.py:27
  134.8 42.9 %copy-start.3 = (f32[16,1,128,128]{3,2,1,0:T(8,128)S(1)}, f32[16,1,128,128]{3,2,1,0:T(8,128)}, u32[]{:S(2)}) copy-start(f32[16,1,128,128]{3,2,1,0:T(8,128)} %all-gather.8.cloned.1.call-done) | copy-start | bytes 3145732
  138.6 39.0 %copy-start.4 = (f32[4,1,128,128]{3,2,1,0:T(8,128)S(1)}, f32[4,1,128,128]{3,2,1,0:T(8,128)}, u32[]{:S(2)}) copy-start(f32[4,1,128,128]{3,2,1,0:T(8,128)} %slice_add_fusion.8) | copy-start | bytes 786436
  160.1 25.5 %copy-start.13 = (f32[128]{0:T(128)S(1)}, f32[128]{0:T(128)}, u32[]{:S(2)}) copy-start(f32[128]{0:T(128)} %param.19) | copy-start | bytes 1540
  206.0 3.7 %copy-start.12 = (f32[2048]{0:T(1024)S(1)}, f32[2048]{0:T(1024)}, u32[]{:S(2)}) copy-start(f32[2048]{0:T(1024)} %param.21) | copy-start | bytes 24580
Sparse Core Ops, SparseCore 0:
  104.6 30.1 all-gather.7
  138.8 38.8 all-gather.5
